TPU v7x, 32 devices: a whole 2x2x4 slice. The times are simulated.
32 devices in a mesh: gr: 2 (over x), fs: 8 (over z, y), tp: 2 (over core).
Axes of the slice: x: 2, y: 2, z: 4, core: 2. Of those that a mesh axis runs over, the one named last changes fastest.
Arguments:
- tokens: bfloat16 [4, 2048, 2048], P(('gr', 'tp')), may hold values from -6 to 6
- gate_master: float32 [3, 2048, 7168], P(None, 'fs', ('gr', 'tp')), may hold values from -0.125 to 0.125
- up_master: float32 [3, 2048, 7168], P(None, 'fs', ('gr', 'tp')), may hold values from -0.125 to 0.125
- down_master: float32 [3, 7168, 2048], P(None, 'fs', ('gr', 'tp')), may hold values from -0.0625 to 0.0625
- norm_gain: float32 [2048], P('fs'), may hold values from 0.1 to 1.9
- route: int32 [4, 2048, 2], P(('gr', 'tp')), may hold values from 0 to 2, all different within a row
- route_weight: float32 [4, 2048, 2], P(('gr', 'tp')), may hold values from 0.05 to 1
Outputs:
- gate_out: bfloat16 [3, 2048, 7168], P(None, None, 'fs')
- up_out: bfloat16 [3, 2048, 7168], P(None, None, 'fs')
- down_out: bfloat16 [3, 7168, 2048], P(None, 'fs')
- mixed: bfloat16 [4, 2048, 2048], P(('gr', 'tp'), 'fs')
Inputs may be any that keep to these rules, and one draw needn't show every extreme that they name: `route`: each token names two different experts; every expert is named by some token.
All inputs are finite; a program needn't handle non-finite values.
Results may differ from a plain program's by a relative error of at most 0.024.
Values may be sent and summed in bfloat16 or wider, within the bound.
A program may use at most 192 MiB of HBM per device.

v0:
```python
import jax
import jax.numpy as jnp
from jax import lax
from jax.sharding import PartitionSpec as P

CHUNKS = 2
GROUP = ("gr", "tp")


def normalize(rows_in):
    values = rows_in.astype(jnp.float32)
    scaled = values * lax.rsqrt(jnp.mean(values * values, axis=-1, keepdims=True) + 1e-06)
    return scaled.astype(jnp.bfloat16)


def mixing(chosen, weights, experts):
    share = weights / jnp.sum(weights, axis=-1, keepdims=True)
    labels = jnp.arange(experts, dtype=jnp.int32)
    match = (chosen[:, :, None] == labels[None, None, :]).astype(jnp.float32)
    return jnp.sum(share[:, :, None] * match, axis=1)


def expert_term(normed, mix_column, gate_weight, up_weight, down_weight):
    gate_act = jnp.dot(normed, gate_weight, preferred_element_type=jnp.float32)
    up_act = jnp.dot(normed, up_weight, preferred_element_type=jnp.float32)
    hidden = (jax.nn.silu(gate_act) * up_act).astype(jnp.bfloat16)
    projected = jnp.dot(hidden, down_weight, preferred_element_type=jnp.float32)
    return mix_column * projected


def make_shards(n_fs, n_group):
    def by_chunks(rows):
        parts = rows.reshape(n_fs, CHUNKS, -1, rows.shape[-1])
        return parts.transpose(1, 0, 2, 3).reshape(rows.shape)

    def shards(tokens, gate_master, up_master, down_master, norm_gain, route, route_weight):
        experts, depth, columns = gate_master.shape
        blocks = n_fs // n_group
        width = columns // blocks
        rows = depth // n_group

        down_local = down_master.astype(jnp.bfloat16)
        down_local, gate_master, up_master = lax.optimization_barrier((down_local, gate_master, up_master))
        down_list = [lax.all_gather(down_local[index], GROUP, axis=1, tiled=True) for index in range(experts)]

        def local(master, index):
            scaled = (norm_gain[:, None] * master[index]).astype(jnp.bfloat16)
            return scaled.reshape(n_group, rows, blocks, width).transpose(0, 2, 1, 3)

        me = lax.axis_index("fs")

        def permuted(sent):
            got = [lax.dynamic_index_in_dim(sent, me, 0, keepdims=True)]
            for shift in range(1, n_fs):
                block = lax.dynamic_index_in_dim(sent, lax.rem(me + shift, n_fs), 0, keepdims=True)
                got.append(lax.ppermute(block, "fs", [(i, (i + shift) % n_fs) for i in range(n_fs)]))
            return got

        def gathered(got):
            mine = jnp.zeros((n_fs,) + got[0].shape[1:], got[0].dtype)
            for shift in range(n_fs):
                source = lax.rem(me - shift + n_fs, n_fs)
                mine = lax.dynamic_update_slice_in_dim(mine, got[shift], source, 0)
            return tuple(
                lax.all_gather(mine[:, which], GROUP, axis=1, tiled=True).reshape(n_fs * depth, width)
                for which in range(2)
            )

        pair = jnp.stack([local(m, i) for i in range(experts) for m in (gate_master, up_master)], axis=2)
        pair = lax.all_to_all(pair, GROUP, split_axis=0, concat_axis=0, tiled=True)
        pair = pair.reshape(n_fs, 2 * experts, rows, width)

        got = [permuted(pair[:, 2 * index : 2 * index + 2]) for index in range(experts)]
        got[0], down_list = lax.optimization_barrier((got[0], down_list))

        normed = by_chunks(normalize(tokens[0]))
        combine = by_chunks(mixing(route[0], route_weight[0], experts))
        total = jnp.zeros(normed.shape, jnp.float32)
        weights = [gathered(got[index]) for index in range(min(2, experts))]
        for index in range(experts - 1):
            total = total + expert_term(
                normed, combine[:, index : index + 1], *weights[index], down_list[index]
            )
            if index + 2 < experts:
                got[index + 2], total = lax.optimization_barrier((got[index + 2], total))
                weights.append(gathered(got[index + 2]))
        last = experts - 1
        size = normed.shape[0] // CHUNKS
        mixed = []
        for chunk in range(CHUNKS):
            part = slice(chunk * size, (chunk + 1) * size)
            summed = total[part] + expert_term(
                normed[part], combine[part, last : last + 1], *weights[last], down_list[last]
            )
            summed = summed.astype(jnp.bfloat16)
            mixed.append(lax.psum_scatter(summed, "fs", scatter_dimension=0, tiled=True))
        weights, down_list, _ = lax.optimization_barrier((weights, down_list, summed))
        gate_out = jnp.stack([pair[0] for pair in weights], axis=0)
        up_out = jnp.stack([pair[1] for pair in weights], axis=0)
        down_out = jnp.stack(down_list, axis=0)
        return (gate_out, up_out, down_out, jnp.concatenate(mixed, axis=0)[None])

    return shards


def solution(mesh):
    n_fs = mesh.shape["fs"]
    n_group = mesh.shape["gr"] * mesh.shape["tp"]
    in_specs = (
        P(GROUP, None, None),
        P(None, "fs", GROUP),
        P(None, "fs", GROUP),
        P(None, "fs", GROUP),
        P("fs"),
        P(GROUP, None, None),
        P(GROUP, None, None),
    )
    out_specs = (
        P(None, None, "fs"),
        P(None, None, "fs"),
        P(None, "fs", None),
        P(GROUP, "fs", None),
    )
    return jax.shard_map(
        make_shards(n_fs, n_group), mesh=mesh, in_specs=in_specs, out_specs=out_specs, check_vma=False
    )
```

profile of v0, /device:TPU:26, one launch (start us, length us, event | category | flops | bytes accessed | tf_op | source)
XLA Modules:
  0.0 610.6 jit_solution(14788001675067907595)
XLA Ops:
  13.2 7.9 %fusion.25 = (f32[1,256,1792]{2,1,0:T(8,128)}, f32[1,256,1792]{2,1,0:T(8,128)S(1)}, f32[1,256,1792]{2,1,0:T(8,128)}, f32[1,256,1792]{2,1,0:T(8,128)}, f32[1,256,1792]{2,1,0:T(8,128)}, /*index=5*/f32[1,256,1792]{2,1,0:T(8,128)}) fusion(f32[3,256,1792]{2,1,0:T(8,128)} %param.9, f32[3,256,1792]{2,1,0:T(8,128)} %param.8), kind=kLoop, calls=%fused_computation.97 | loop fusion | bytes 22020096 | tf_op jit(solution)/shard_map/slice | solution.py:47
  21.2 3.5 squeeze.49
  24.8 3.2 squeeze.50
  28.0 3.2 squeeze.51
  35.8 3.3 fusion.7
  51.1 5.8 all-to-all-start
  57.4 96.3 %all-to-all-done = bf16[4,2,6,64,896]{4,1,3,2,0:T(2,128)(2,1)} async-done(((bf16[4,2,6,64,896]{4,1,3,2,0:T(2,128)(2,1)}), bf16[4,2,6,64,896]{4,1,3,2,0:T(2,128)(2,1)}, u32[]{:S(2)}, u32[]{:S(2)}) %all-to-all-start) | async-done | bytes 5505056 | tf_op jit(solution)/shard_map/all_to_all | solution.py:70
  153.7 3.7 copy.48
  170.1 24.5 %collective-permute-start.6 = (bf16[1,2,64,896]{3,2,1,0:T(8,128)(2,1)}, bf16[1,2,64,896]{3,2,1,0:T(8,128)(2,1)}, u32[]{:S(2)}, u32[]{:S(2)}) collective-permute-start(bf16[1,2,64,896]{3,2,1,0:T(8,128)(2,1)} %get-tuple-element.104), channel_id=1, source_target_pairs={{0,14},{2,0},{4,2},{6,4},{8,6},{10,8},{12,10},{14,12},{1,15},{3,1}... | collective-permute-start | bytes 688136 | tf_op jit(solution)/shard_map/ppermute | solution.py:56
  194.7 4.4 collective-permute-done.2
  203.8 5.3 collective-permute-start.7
  217.5 24.0 %collective-permute-start.13 = (bf16[1,2,64,896]{3,2,1,0:T(8,128)(2,1)S(1)}, bf16[1,2,64,896]{3,2,1,0:T(8,128)(2,1)S(1)}, u32[]{:S(2)}, u32[]{:S(2)}) collective-permute-start(bf16[1,2,64,896]{3,2,1,0:T(8,128)(2,1)S(1)} %get-tuple-element.94), channel_id=1, source_target_pairs={{0,14},{2,0},{4,2},{6,4},{8,6},{10,8},{12,10},{14,12},{1,15},{3,1}... | collective-permute-start | bytes 688136 | tf_op jit(solution)/shard_map/ppermute | solution.py:56
  241.6 4.3 collective-permute-done.9
  248.1 5.8 multiply_reduce_fusion
  254.0 8.2 %fusion = bf16[2,8,128,2048]{3,2,0,1:T(8,128)(2,1)} fusion(f32[8,2,128]{2,1,0:T(2,128)S(1)} %bitcast.148, bf16[8,2,128,2048]{3,2,1,0:T(8,128)(2,1)} %bitcast.116), kind=kLoop, calls=%fused_computation.7 | loop fusion | flops 12582912 | bytes 16785408 | tf_op jit(solution)/shard_map/transpose | solution.py:34
  262.2 8.6 %copy.50 = bf16[2,8,128,2048]{3,2,1,0:T(8,128)(2,1)} copy(bf16[2,8,128,2048]{3,2,0,1:T(8,128)(2,1)} %fusion) | data formatting | bytes 16777216 | tf_op jit(solution)/shard_map/transpose | solution.py:34
  272.0 4.6 collective-permute-start.14
  281.1 14.9 %fusion.33 = f32[2048,896]{1,0:T(8,128)} fusion(bf16[2048,2048]{1,0:T(8,128)(2,1)} %bitcast.118, bf16[2048,896]{1,0:T(8,128)(2,1)} %bitcast.130), kind=kOutput, calls=%fused_computation.105 | convolution fusion | flops 7516192768 | bytes 19398656 | tf_op jit(solution)/shard_map/dot_general | solution.py:24
  298.9 26.8 %convolution_multiply_fusion = f32[2048,2048]{1,0:T(8,128)} fusion(bf16[896,2048]{1,0:T(8,128)(2,1)} %bitcast.126, f32[2048]{0:T(1024)S(1)} %bitcast.151, f32[2048,896]{1,0:T(8,128)} %fusion.33, bf16[2048,2048]{1,0:T(8,128)(2,1)} %bitcast.119, bf16[2048,896]{1,0:T(8,128)(2,1)} %bitcast.132), kind=kOutput, calls=%fused_computation.6 | convolution fusion | flops 15047589888 | bytes 39854080 | tf_op jit(solution)/shard_map/dot_general | solution.py:27
  328.1 6.2 %fusion.23 = (bf16[1,8,128,2048]{3,2,0,1:T(8,128)(2,1)}, bf16[1,8,128,2048]{3,2,0,1:T(8,128)(2,1)}) fusion(bf16[2,8,128,2048]{3,2,0,1:T(8,128)(2,1)} %fusion), kind=kLoop, calls=%fused_computation.95 | loop fusion | bytes 16777216 | tf_op jit(solution)/shard_map/slice | solution.py:93
  334.3 14.2 %fusion.34 = f32[2048,896]{1,0:T(8,128)} fusion(bf16[2048,2048]{1,0:T(8,128)(2,1)} %bitcast.120, bf16[2048,896]{1,0:T(8,128)(2,1)} %bitcast.134), kind=kOutput, calls=%fused_computation.106 | convolution fusion | flops 7516192768 | bytes 19398656 | tf_op jit(solution)/shard_map/dot_general | solution.py:24
  348.6 27.0 %fusion.3 = f32[2048,2048]{1,0:T(8,128)} fusion(bf16[896,2048]{1,0:T(8,128)(2,1)} %bitcast.127, f32[2048,896]{1,0:T(8,128)} %fusion.34, bf16[2048,2048]{1,0:T(8,128)(2,1)} %bitcast.121, bf16[2048,896]{1,0:T(8,128)(2,1)} %bitcast.136), kind=kOutput, calls=%fused_computation.14 | convolution fusion | flops 15043395584 | bytes 39845888 | tf_op jit(solution)/shard_map/dot_general | solution.py:27
  375.6 18.8 %multiply_add_fusion = f32[2048,2048]{1,0:T(8,128)} fusion(f32[2048,2048]{1,0:T(8,128)} %convolution_multiply_fusion, f32[2048,2048]{1,0:T(8,128)} %fusion.3, f32[2048]{0:T(1024)S(1)} %bitcast.149), kind=kLoop, calls=%fused_computation | loop fusion | flops 8388608 | bytes 50339840 | tf_op jit(solution)/shard_map/add | solution.py:81
  394.4 9.7 %fusion.36 = f32[1024,896]{1,0:T(8,128)} fusion(bf16[1024,2048]{1,0:T(8,128)(2,1)} %bitcast.124, bf16[2048,896]{1,0:T(8,128)(2,1)} %bitcast.138), kind=kOutput, calls=%fused_computation.108 | convolution fusion | flops 3758096384 | bytes 11534336 | tf_op jit(solution)/shard_map/dot_general | solution.py:24
  404.3 17.3 %fusion.1 = bf16[1024,2048]{1,0:T(8,128)(2,1)} fusion(f32[2048,2048]{1,0:T(8,128)} %multiply_add_fusion, bf16[896,2048]{1,0:T(8,128)(2,1)} %bitcast.128, f32[1024]{0:T(1024)S(1)} %bitcast.153, f32[1024,896]{1,0:T(8,128)} %fusion.36, bf16[1024,2048]{1,0:T(8,128)(2,1)} %bitcast.125, bf16[2048,896]{1,0:T(8,128)(2,1)} %bitcast.141), kind=kOutput, calls=%fused_computation.9 | convolution fusion | flops 7527989248 | bytes 27791360 | tf_op jit(solution)/shard_map/dot_general | solution.py:27
  421.7 9.6 %fusion.35 = f32[1024,896]{1,0:T(8,128)} fusion(bf16[1024,2048]{1,0:T(8,128)(2,1)} %bitcast.122, bf16[2048,896]{1,0:T(8,128)(2,1)} %bitcast.139), kind=kOutput, calls=%fused_computation.107 | convolution fusion | flops 3758096384 | bytes 11534336 | tf_op jit(solution)/shard_map/dot_general | solution.py:24
  431.3 16.5 %fusion.2 = bf16[1024,2048]{1,0:T(8,128)(2,1)} fusion(f32[2048,2048]{1,0:T(8,128)} %multiply_add_fusion, bf16[896,2048]{1,0:T(8,128)(2,1)} %bitcast.129, f32[1024]{0:T(1024)S(1)} %bitcast.152, f32[1024,896]{1,0:T(8,128)} %fusion.35, bf16[1024,2048]{1,0:T(8,128)(2,1)} %bitcast.123, bf16[2048,896]{1,0:T(8,128)(2,1)} %bitcast.142), kind=kOutput, calls=%fused_computation.11 | convolution fusion | flops 7527989248 | bytes 27791360 | tf_op jit(solution)/shard_map/dot_general | solution.py:27
  447.9 11.8 %pad_maximum_fusion.2 = bf16[3,896,2048]{2,1,0:T(8,128)(2,1)} fusion(bf16[1,896,2048]{2,1,0:T(8,128)(2,1)} %all-gather.23.cloned.1.call-done, bf16[1,896,2048]{2,1,0:T(8,128)(2,1)} %all-gather.21.cloned.1.call-done, bf16[1,896,2048]{2,1,0:T(8,128)(2,1)} %all-gather.19.cloned.1.call-done), kind=kLoop, calls=%fused_computation.5 | loop fusion | flops 11010048 | bytes 22020096 | tf_op jit(solution)/shard_map/stack | solution.py:100
  459.8 5.8 pad_maximum_fusion.1
  467.8 5.0 pad_maximum_fusion
  472.8 36.9 %reduce-scatter.3.cloned.1.call-done = bf16[128,2048]{1,0:T(8,128)(2,1)} async-done(((bf16[1024,2048]{1,0:T(8,128)(2,1)}), bf16[128,2048]{1,0:T(8,128)(2,1)}) %reduce-scatter.3.cloned.1.call-update) | async-done | bytes 524304 | tf_op jit(solution)/shard_map/reduce_scatter | solution.py:96
  509.7 91.6 %reduce-scatter.5.cloned.1.call-done = bf16[128,2048]{1,0:T(8,128)(2,1)} async-done(((bf16[1024,2048]{1,0:T(8,128)(2,1)}), bf16[128,2048]{1,0:T(8,128)(2,1)}) %reduce-scatter.5.cloned.1.call-update) | async-done | bytes 524304 | tf_op jit(solution)/shard_map/reduce_scatter | solution.py:96
  (146 shorter events, 66.9 us)
Async XLA Ops:
  7.2 192.5 %all-gather.19.cloned.1.call-start = ((), (), s32[]{:S(2)}) async-start(), calls=%async_computation.5 | async-start | bytes 4587520 | tf_op jit(solution)/shard_map/all_gather | solution.py:44
  11.7 187.9 %all-gather.21.cloned.1.call-start = ((), (), s32[]{:S(2)}) async-start(), calls=%async_computation.6 | async-start | bytes 4587520 | tf_op jit(solution)/shard_map/all_gather | solution.py:44
  12.5 187.2 %all-gather.23.cloned.1.call-start = ((), (), s32[]{:S(2)}) async-start(), calls=%async_computation.7 | async-start | bytes 4587520 | tf_op jit(solution)/shard_map/all_gather | solution.py:44
  51.1 102.6 %all-to-all-start = ((bf16[4,2,6,64,896]{4,1,3,2,0:T(2,128)(2,1)}), bf16[4,2,6,64,896]{4,1,3,2,0:T(2,128)(2,1)}, u32[]{:S(2)}, u32[]{:S(2)}) async-start(bf16[4,2,6,64,896]{4,1,3,2,0:T(2,128)(2,1)} %fusion.17), calls=%async_computation | async-start | bytes 11010048 | tf_op jit(solution)/shard_map/all_to_all | solution.py:70
  56.9 224.2 %all-gather.25.cloned.1.call-start = ((), (), s32[]{:S(2)}) async-start(), calls=%async_computation.8 | async-start | bytes 4587520 | tf_op jit(solution)/shard_map/all_gather | solution.py:65
  160.2 9.4 %collective-permute-start = (bf16[1,2,64,896]{3,2,1,0:T(8,128)(2,1)S(1)}, bf16[1,2,64,896]{3,2,1,0:T(8,128)(2,1)S(1)}, u32[]{:S(2)}, u32[]{:S(2)}) collective-permute-start(bf16[1,2,64,896]{3,2,1,0:T(8,128)(2,1)S(1)} %get-tuple-element.110), channel_id=1, source_target_pairs={{0,2},{2,4},{4,6},{6,8},{8,10},{10,12},{12,14},{14,0},{1,3},{3,5},... | collective-permute-start | bytes 688136 | tf_op jit(solution)/shard_map/ppermute | solution.py:56
  161.7 8.5 %collective-permute-start.1 = (bf16[1,2,64,896]{3,2,1,0:T(8,128)(2,1)S(1)}, bf16[1,2,64,896]{3,2,1,0:T(8,128)(2,1)S(1)}, u32[]{:S(2)}, u32[]{:S(2)}) collective-permute-start(bf16[1,2,64,896]{3,2,1,0:T(8,128)(2,1)S(1)} %get-tuple-element.109), channel_id=1, source_target_pairs={{0,4},{2,6},{4,8},{6,10},{8,12},{10,14},{12,0},{14,2},{1,5},{3,7},... | collective-permute-start | bytes 688136 | tf_op jit(solution)/shard_map/ppermute | solution.py:56
  162.2 36.9 %collective-permute-start.2 = (bf16[1,2,64,896]{3,2,1,0:T(8,128)(2,1)}, bf16[1,2,64,896]{3,2,1,0:T(8,128)(2,1)S(1)}, u32[]{:S(2)}, u32[]{:S(2)}) collective-permute-start(bf16[1,2,64,896]{3,2,1,0:T(8,128)(2,1)} %get-tuple-element.108), channel_id=1, source_target_pairs={{0,6},{2,8},{4,10},{6,12},{8,14},{10,0},{12,2},{14,4},{1,7},{3,9},... | collective-permute-start | bytes 688136 | tf_op jit(solution)/shard_map/ppermute | solution.py:56
  164.5 35.1 %collective-permute-start.3 = (bf16[1,2,64,896]{3,2,1,0:T(8,128)(2,1)}, bf16[1,2,64,896]{3,2,1,0:T(8,128)(2,1)S(1)}, u32[]{:S(2)}, u32[]{:S(2)}) collective-permute-start(bf16[1,2,64,896]{3,2,1,0:T(8,128)(2,1)} %get-tuple-element.107), channel_id=1, source_target_pairs={{0,8},{2,10},{4,12},{6,14},{8,0},{10,2},{12,4},{14,6},{1,9},{3,11}... | collective-permute-start | bytes 688136 | tf_op jit(solution)/shard_map/ppermute | solution.py:56
  164.9 34.7 %collective-permute-start.4 = (bf16[1,2,64,896]{3,2,1,0:T(8,128)(2,1)}, bf16[1,2,64,896]{3,2,1,0:T(8,128)(2,1)S(1)}, u32[]{:S(2)}, u32[]{:S(2)}) collective-permute-start(bf16[1,2,64,896]{3,2,1,0:T(8,128)(2,1)} %get-tuple-element.106), channel_id=1, source_target_pairs={{0,10},{2,12},{4,14},{6,0},{8,2},{10,4},{12,6},{14,8},{1,11},{3,13... | collective-permute-start | bytes 688136 | tf_op jit(solution)/shard_map/ppermute | solution.py:56
  169.6 30.1 %collective-permute-start.5 = (bf16[1,2,64,896]{3,2,1,0:T(8,128)(2,1)}, bf16[1,2,64,896]{3,2,1,0:T(8,128)(2,1)S(1)}, u32[]{:S(2)}, u32[]{:S(2)}) collective-permute-start(bf16[1,2,64,896]{3,2,1,0:T(8,128)(2,1)} %get-tuple-element.105), channel_id=1, source_target_pairs={{0,12},{2,14},{4,0},{6,2},{8,4},{10,6},{12,8},{14,10},{1,13},{3,15... | collective-permute-start | bytes 688136 | tf_op jit(solution)/shard_map/ppermute | solution.py:56
  170.1 29.5 %collective-permute-start.6 = (bf16[1,2,64,896]{3,2,1,0:T(8,128)(2,1)}, bf16[1,2,64,896]{3,2,1,0:T(8,128)(2,1)}, u32[]{:S(2)}, u32[]{:S(2)}) collective-permute-start(bf16[1,2,64,896]{3,2,1,0:T(8,128)(2,1)} %get-tuple-element.104), channel_id=1, source_target_pairs={{0,14},{2,0},{4,2},{6,4},{8,6},{10,8},{12,10},{14,12},{1,15},{3,1}... | collective-permute-start | bytes 688136 | tf_op jit(solution)/shard_map/ppermute | solution.py:56
  202.6 96.2 %all-gather.27.cloned.1.call-start = ((), (), s32[]{:S(2)}) async-start(), calls=%async_computation.9 | async-start | bytes 4587520 | tf_op jit(solution)/shard_map/all_gather | solution.py:65
  203.2 131.1 %all-gather.29.cloned.1.call-start = ((), (), s32[]{:S(2)}) async-start(), calls=%async_computation.10 | async-start | bytes 4587520 | tf_op jit(solution)/shard_map/all_gather | solution.py:65
  203.8 10.6 %collective-permute-start.7 = (bf16[1,2,64,896]{3,2,1,0:T(8,128)(2,1)S(1)}, bf16[1,2,64,896]{3,2,1,0:T(8,128)(2,1)S(1)}, u32[]{:S(2)}, u32[]{:S(2)}) collective-permute-start(bf16[1,2,64,896]{3,2,1,0:T(8,128)(2,1)S(1)} %get-tuple-element.100), channel_id=1, source_target_pairs={{0,2},{2,4},{4,6},{6,8},{8,10},{10,12},{12,14},{14,0},{1,3},{3,5},... | collective-permute-start | bytes 688136 | tf_op jit(solution)/shard_map/ppermute | solution.py:56
  209.0 36.9 %collective-permute-start.9 = (bf16[1,2,64,896]{3,2,1,0:T(8,128)(2,1)S(1)}, bf16[1,2,64,896]{3,2,1,0:T(8,128)(2,1)S(1)}, u32[]{:S(2)}, u32[]{:S(2)}) collective-permute-start(bf16[1,2,64,896]{3,2,1,0:T(8,128)(2,1)S(1)} %get-tuple-element.98), channel_id=1, source_target_pairs={{0,6},{2,8},{4,10},{6,12},{8,14},{10,0},{12,2},{14,4},{1,7},{3,9},... | collective-permute-start | bytes 688136 | tf_op jit(solution)/shard_map/ppermute | solution.py:56
  211.5 35.0 %collective-permute-start.10 = (bf16[1,2,64,896]{3,2,1,0:T(8,128)(2,1)S(1)}, bf16[1,2,64,896]{3,2,1,0:T(8,128)(2,1)S(1)}, u32[]{:S(2)}, u32[]{:S(2)}) collective-permute-start(bf16[1,2,64,896]{3,2,1,0:T(8,128)(2,1)S(1)} %get-tuple-element.97), channel_id=1, source_target_pairs={{0,8},{2,10},{4,12},{6,14},{8,0},{10,2},{12,4},{14,6},{1,9},{3,11}... | collective-permute-start | bytes 688136 | tf_op jit(solution)/shard_map/ppermute | solution.py:56
  212.0 34.5 %collective-permute-start.11 = (bf16[1,2,64,896]{3,2,1,0:T(8,128)(2,1)S(1)}, bf16[1,2,64,896]{3,2,1,0:T(8,128)(2,1)S(1)}, u32[]{:S(2)}, u32[]{:S(2)}) collective-permute-start(bf16[1,2,64,896]{3,2,1,0:T(8,128)(2,1)S(1)} %get-tuple-element.96), channel_id=1, source_target_pairs={{0,10},{2,12},{4,14},{6,0},{8,2},{10,4},{12,6},{14,8},{1,11},{3,13... | collective-permute-start | bytes 688136 | tf_op jit(solution)/shard_map/ppermute | solution.py:56
  214.3 32.2 %collective-permute-start.12 = (bf16[1,2,64,896]{3,2,1,0:T(8,128)(2,1)S(1)}, bf16[1,2,64,896]{3,2,1,0:T(8,128)(2,1)S(1)}, u32[]{:S(2)}, u32[]{:S(2)}) collective-permute-start(bf16[1,2,64,896]{3,2,1,0:T(8,128)(2,1)S(1)} %get-tuple-element.95), channel_id=1, source_target_pairs={{0,12},{2,14},{4,0},{6,2},{8,4},{10,6},{12,8},{14,10},{1,13},{3,15... | collective-permute-start | bytes 688136 | tf_op jit(solution)/shard_map/ppermute | solution.py:56
  217.5 29.1 %collective-permute-start.13 = (bf16[1,2,64,896]{3,2,1,0:T(8,128)(2,1)S(1)}, bf16[1,2,64,896]{3,2,1,0:T(8,128)(2,1)S(1)}, u32[]{:S(2)}, u32[]{:S(2)}) collective-permute-start(bf16[1,2,64,896]{3,2,1,0:T(8,128)(2,1)S(1)} %get-tuple-element.94), channel_id=1, source_target_pairs={{0,14},{2,0},{4,2},{6,4},{8,6},{10,8},{12,10},{14,12},{1,15},{3,1}... | collective-permute-start | bytes 688136 | tf_op jit(solution)/shard_map/ppermute | solution.py:56
  248.1 100.5 %all-gather.31.cloned.1.call-start = ((), (), s32[]{:S(2)}) async-start(), calls=%async_computation.11 | async-start | bytes 4587520 | tf_op jit(solution)/shard_map/all_gather | solution.py:65
  272.0 23.9 %collective-permute-start.14 = (bf16[1,2,64,896]{3,2,1,0:T(8,128)(2,1)}, bf16[1,2,64,896]{3,2,1,0:T(8,128)(2,1)S(1)}, u32[]{:S(2)}, u32[]{:S(2)}) collective-permute-start(bf16[1,2,64,896]{3,2,1,0:T(8,128)(2,1)} %get-tuple-element.90), channel_id=1, source_target_pairs={{0,2},{2,4},{4,6},{6,8},{8,10},{10,12},{12,14},{14,0},{1,3},{3,5},... | collective-permute-start | bytes 688136 | tf_op jit(solution)/shard_map/ppermute | solution.py:56
  276.6 20.8 %collective-permute-start.15 = (bf16[1,2,64,896]{3,2,1,0:T(8,128)(2,1)S(1)}, bf16[1,2,64,896]{3,2,1,0:T(8,128)(2,1)S(1)}, u32[]{:S(2)}, u32[]{:S(2)}) collective-permute-start(bf16[1,2,64,896]{3,2,1,0:T(8,128)(2,1)S(1)} %get-tuple-element.89), channel_id=1, source_target_pairs={{0,4},{2,6},{4,8},{6,10},{8,12},{10,14},{12,0},{14,2},{1,5},{3,7},... | collective-permute-start | bytes 688136 | tf_op jit(solution)/shard_map/ppermute | solution.py:56
  276.6 49.0 %collective-permute-start.16 = (bf16[1,2,64,896]{3,2,1,0:T(8,128)(2,1)S(1)}, bf16[1,2,64,896]{3,2,1,0:T(8,128)(2,1)S(1)}, u32[]{:S(2)}, u32[]{:S(2)}) collective-permute-start(bf16[1,2,64,896]{3,2,1,0:T(8,128)(2,1)S(1)} %get-tuple-element.88), channel_id=1, source_target_pairs={{0,6},{2,8},{4,10},{6,12},{8,14},{10,0},{12,2},{14,4},{1,7},{3,9},... | collective-permute-start | bytes 688136 | tf_op jit(solution)/shard_map/ppermute | solution.py:56
  277.9 47.8 %collective-permute-start.17 = (bf16[1,2,64,896]{3,2,1,0:T(8,128)(2,1)S(1)}, bf16[1,2,64,896]{3,2,1,0:T(8,128)(2,1)S(1)}, u32[]{:S(2)}, u32[]{:S(2)}) collective-permute-start(bf16[1,2,64,896]{3,2,1,0:T(8,128)(2,1)S(1)} %get-tuple-element.87), channel_id=1, source_target_pairs={{0,8},{2,10},{4,12},{6,14},{8,0},{10,2},{12,4},{14,6},{1,9},{3,11}... | collective-permute-start | bytes 688136 | tf_op jit(solution)/shard_map/ppermute | solution.py:56
  279.6 46.1 %collective-permute-start.18 = (bf16[1,2,64,896]{3,2,1,0:T(8,128)(2,1)S(1)}, bf16[1,2,64,896]{3,2,1,0:T(8,128)(2,1)S(1)}, u32[]{:S(2)}, u32[]{:S(2)}) collective-permute-start(bf16[1,2,64,896]{3,2,1,0:T(8,128)(2,1)S(1)} %get-tuple-element.86), channel_id=1, source_target_pairs={{0,10},{2,12},{4,14},{6,0},{8,2},{10,4},{12,6},{14,8},{1,11},{3,13... | collective-permute-start | bytes 688136 | tf_op jit(solution)/shard_map/ppermute | solution.py:56
  280.8 113.6 %all-gather.33.cloned.1.call-start = ((), (), s32[]{:S(2)}) async-start(), calls=%async_computation.12 | async-start | bytes 4587520 | tf_op jit(solution)/shard_map/all_gather | solution.py:65
  295.9 29.7 %collective-permute-start.19 = (bf16[1,2,64,896]{3,2,1,0:T(8,128)(2,1)S(1)}, bf16[1,2,64,896]{3,2,1,0:T(8,128)(2,1)S(1)}, u32[]{:S(2)}, u32[]{:S(2)}) collective-permute-start(bf16[1,2,64,896]{3,2,1,0:T(8,128)(2,1)S(1)} %get-tuple-element.85), channel_id=1, source_target_pairs={{0,12},{2,14},{4,0},{6,2},{8,4},{10,6},{12,8},{14,10},{1,13},{3,15... | collective-permute-start | bytes 688136 | tf_op jit(solution)/shard_map/ppermute | solution.py:56
  297.4 28.2 %collective-permute-start.20 = (bf16[1,2,64,896]{3,2,1,0:T(8,128)(2,1)S(1)}, bf16[1,2,64,896]{3,2,1,0:T(8,128)(2,1)S(1)}, u32[]{:S(2)}, u32[]{:S(2)}) collective-permute-start(bf16[1,2,64,896]{3,2,1,0:T(8,128)(2,1)S(1)} %get-tuple-element.84), channel_id=1, source_target_pairs={{0,14},{2,0},{4,2},{6,4},{8,6},{10,8},{12,10},{14,12},{1,15},{3,1}... | collective-permute-start | bytes 688136 | tf_op jit(solution)/shard_map/ppermute | solution.py:56
  327.8 76.5 %all-gather.35.cloned.1.call-start = ((), (), s32[]{:S(2)}) async-start(), calls=%async_computation.13 | async-start | bytes 4587520 | tf_op jit(solution)/shard_map/all_gather | solution.py:65
  348.5 161.2 %reduce-scatter.3.cloned.1.call-start = ((), (), s32[]{:S(2)}) async-start(), calls=%async_computation.3 | async-start | bytes 4718592 | tf_op jit(solution)/shard_map/reduce_scatter | solution.py:96
  421.6 179.7 %reduce-scatter.5.cloned.1.call-start = ((), (), s32[]{:S(2)}) async-start(), calls=%async_computation.4 | async-start | bytes 4718592 | tf_op jit(solution)/shard_map/reduce_scatter | solution.py:96
  (13 other events, 109.3 us)
Sparse Core Ops, SparseCore 0:
  11.9 31.5 all-gather.18
  45.0 48.1 all-gather.20
  95.3 51.1 all-gather.22
  202.8 35.1 all-gather.24
  240.0 31.4 all-gather.26
  272.9 31.4 all-gather.28
  306.0 31.4 all-gather.30
  339.1 31.4 all-gather.32
  372.7 31.4 all-gather.34
  421.7 87.9 reduce-scatter.2
  513.3 87.9 reduce-scatter.4
where the time goes:
time: 623 us; the launch traced here: 611 us
  waiting for transfers between devices  240 us (39%)
  matrix products  136 us (22%)
  starting transfers between devices  88.4 us (14%)
  other arithmetic  73.8 us (12%)
  local copies, waits for them, and re-layouts  58 us (9%)
  between operations  14.8 us (2%)
    reduce_scatter x2, waiting for transfers between devices, shards(): lax.psum_scatter(summed, 'fs', scatter_dimension=0, tiled=True)  129 us
    all_to_all x1, waiting for transfers between devices, shards(): pair = lax.all_to_all(pair, GROUP, split_axis=0, concat_axis=0, tiled=True)  96.3 us
    dot_general x4, matrix products, expert_term(): projected = jnp.dot(hidden, down_weight, preferred_element_type=jnp.float32)  87.6 us
    ppermute x21, starting transfers between devices, permuted(): lax.ppermute(block, 'fs', [(i, (i + shift) % n_fs) for i in range(n_fs)])  81.3 us
    dot_general x4, matrix products, expert_term(): gate_act = jnp.dot(normed, gate_weight, preferred_element_type=jnp.float32)  48.4 us
    add x1, other arithmetic, shards(): total + expert_term(normed, combine[:, index:index + 1], *weights[index],...  18.8 us
    squeeze x6, local copies, waits for them, and re-layouts, local(): scaled = (norm_gain[:, None] * master[index]).astype(jnp.bfloat16)  16.8 us
  transfers between devices with their start and end apart: 33, of which 10 were waited for; matrix products, arithmetic and copies ran while one was open for 39% of the time, Pallas kernels for 0%

commit v1 on v0

v1 whole, which is shorter than its diff:
```python
import functools

import jax
import jax.numpy as jnp
from jax import lax
from jax.experimental import pallas as pl
from jax.experimental.pallas import tpu as pltpu
from jax.sharding import PartitionSpec as P

GROUP = ("gr", "tp")
MESH = pl.DeviceIdType.MESH
LANES = 128


def mixing(chosen, weights, experts):
    share = weights / jnp.sum(weights, axis=-1, keepdims=True)
    labels = jnp.arange(experts, dtype=jnp.int32)
    match = (chosen[:, :, None] == labels[None, None, :]).astype(jnp.float32)
    return jnp.sum(share[:, :, None] * match, axis=1)


def kernel(
    n_fs, side,
    tok, gate_b, up_b, down_b, comb,
    gate_o, up_o, down_o, mixed_o, stage,
    nrm, total, w1, wd, hid, bounce, dbounce, ysend, yrecv, zsend, zrecv, mout,
    x1s, x1r, z1s, z2s, rl, rs, x2s, d1s, d2s, dxs, dxr, dps, dpr, dfs, dfr, ys, yr, zs, zr, lsem,
):
    gr, s, tp = lax.axis_index("gr"), lax.axis_index("fs"), lax.axis_index("tp")
    src = (gate_b, up_b)
    out = (gate_o, up_o)
    experts, blocks, rows, width = gate_b.shape
    depth = n_fs * rows
    high = down_b.shape[2]
    count, features = tok.shape
    long = rows - side
    tile_rows = count // n_fs
    n_hi = n_fs // 2
    z, y = s // 2, s % 2

    g, other = gr * 2 + tp, (1 - gr) * 2 + tp
    home = s // blocks
    off_plane = (gr - home // 2) * (gr - home // 2)
    off_core = (tp - home % 2) * (tp - home % 2)
    receives = off_core == 0
    lo = side * off_plane
    far_lo = long * off_plane
    back_lo = long * (1 - off_plane)

    across = {"gr": 1 - gr, "fs": s, "tp": tp}
    partner = {"gr": gr, "fs": s, "tp": 1 - tp}

    def along(f):
        return {"gr": gr, "fs": f, "tp": tp}

    def remote(a, b, send, recv, to):
        return pltpu.make_async_remote_copy(
            src_ref=a, dst_ref=b, send_sem=send, recv_sem=recv, device_id=to, device_id_type=MESH
        )

    def window(start, size):
        return pl.ds(pl.multiple_of(start, 16), size)

    def x1(e, m, j):
        u = 2 * e + m
        return remote(
            src[m].at[e, j, pl.ds(side, long)], stage.at[e, m, j], x1s.at[u, j], x1r.at[u, j], across
        )

    def z1(e, m, j):
        u = 2 * e + m
        return remote(
            src[m].at[e, j, pl.ds(0, long)], out[m].at[e, window(s * rows, long)],
            z1s.at[u, j], rl.at[u, s], along(g * blocks + j),
        )

    def z2(e, m, j):
        u = 2 * e + m
        return remote(
            stage.at[e, m, j], out[m].at[e, window(s * rows + side, long)],
            z2s.at[u, j], rl.at[u, s], along(other * blocks + j),
        )

    def long_part(e, m, at):
        return out[m].at[e, window(at * rows + lo, long)]

    def d1(e, m, at):
        u = 2 * e + m
        part = long_part(e, m, at)
        return remote(part, part, d1s.at[u, at], rl.at[u, at], partner)

    def x2(e, m, at):
        u = 2 * e + m
        part = out[m].at[e, window(at * rows + far_lo, side)]
        return remote(part, part, x2s.at[u, at], rs.at[u, at], across)

    def d2(e, m, at):
        u = 2 * e + m
        part = out[m].at[e, window(at * rows + back_lo, side)]
        return remote(part, part, d2s.at[u, at], rs.at[u, at], partner)

    def columns(group):
        return pl.ds(pl.multiple_of(group * high, LANES), high)

    def dx(e):
        return remote(down_b.at[e], down_o.at[e, :, columns(g)], dxs.at[e], dxr.at[e], across)

    def dp(e):
        return remote(down_b.at[e], down_o.at[e, :, columns(g)], dps.at[e], dpr.at[e], partner)

    def df(e):
        part = down_o.at[e, :, columns(other)]
        return remote(part, part, dfs.at[e], dfr.at[e], partner)

    def each(fn):
        lax.fori_loop(0, n_fs, lambda k, c: (fn(k), c)[1], 0)

    def start_x1(e):
        for m in range(2):
            for j in range(blocks):
                x1(e, m, j).start()

    def start_z1(e):
        for m in range(2):
            for j in range(blocks):
                @pl.when(g * blocks + j != s)
                def _():
                    z1(e, m, j).start()

    def start_down(e):
        dx(e).start()
        dp(e).start()

    def relay(e):
        for m in range(2):
            for j in range(blocks):
                x1(e, m, j).wait_recv()

                @pl.when(other * blocks + j != s)
                def _():
                    z2(e, m, j).start()

    def relay_down(e):
        dx(e).wait_recv()
        df(e).start()

    def local(a, buffer, b):
        copy = pltpu.make_async_copy(a, buffer, lsem.at[0])
        copy.start()
        copy.wait()
        copy = pltpu.make_async_copy(buffer, b, lsem.at[0])
        copy.start()
        copy.wait()

    def collect_long(e):
        @pl.when(receives)
        def _():
            for m in range(2):
                mine = s - home * blocks

                @pl.when(off_plane == 0)
                def _():
                    local(src[m].at[e, mine, pl.ds(0, long)], bounce, long_part(e, m, s))

                @pl.when(off_plane != 0)
                def _():
                    local(stage.at[e, m, mine], bounce, long_part(e, m, s))

            def step(k):
                at = lax.rem(s + k, n_fs)
                for m in range(2):
                    @pl.when(k != 0)
                    def _():
                        d1(e, m, at).wait_recv()

                    x2(e, m, at).start()
                    d1(e, m, at).start()

            each(step)

    def collect_short(e):
        @pl.when(receives)
        def _():
            def step(k):
                at = lax.rem(s + k, n_fs)
                for m in range(2):
                    d2(e, m, at).wait_recv()
                    d2(e, m, at).start()

            each(step)

        @pl.when(off_core != 0)
        def _():
            def step(k):
                at = lax.rem(s + k, n_fs)
                for m in range(2):
                    d1(e, m, at).wait_recv()
                    d2(e, m, at).wait_recv()

            each(step)

    fused = width % LANES == 0

    def load(e):
        dp(e).wait_recv()
        df(e).wait_recv()
        copies = [pltpu.make_async_copy(down_o.at[e], wd, lsem.at[1])]
        if fused:
            for c in range(width // LANES):
                for m in range(2):
                    copies.append(
                        pltpu.make_async_copy(
                            out[m].at[e, :, pl.ds(c * LANES, LANES)],
                            w1.at[c, :, pl.ds(m * LANES, LANES)],
                            lsem.at[2 + 2 * c + m],
                        )
                    )
        else:
            for m in range(2):
                copies.append(pltpu.make_async_copy(out[m].at[e], w1.at[m], lsem.at[2 + m]))
        for copy in copies:
            copy.start()
        for copy in copies:
            copy.wait()

    def gated(gate_act, up_act):
        return (gate_act / (1.0 + jnp.exp(-gate_act)) * up_act).astype(jnp.bfloat16)

    def dot(a, b):
        return jnp.dot(a, b, preferred_element_type=jnp.float32)

    step_n = min(512, features)

    def tile(e, t):
        at = window(t * tile_rows, tile_rows)
        if fused:
            def hidden(c, carry):
                both = dot(nrm[at, :], w1[c])
                hid[:, pl.ds(pl.multiple_of(c * LANES, LANES), LANES)] = gated(both[:, :LANES], both[:, LANES:])
                return carry

            lax.fori_loop(0, width // LANES, hidden, 0)
        else:
            hid[...] = gated(dot(nrm[at, :], w1[0]), dot(nrm[at, :], w1[1]))

        def project(c, carry):
            cols = pl.ds(pl.multiple_of(c * step_n, LANES), step_n)
            term = comb[at, e : e + 1] * dot(hid[...], wd[:, cols])
            total[at, cols] = term if e == 0 else total[at, cols] + term
            return carry

        lax.fori_loop(0, features // step_n, project, 0)
        return at

    barrier = pltpu.get_barrier_semaphore()

    def greet(k, c):
        pl.semaphore_signal(barrier, inc=1, device_id=along(lax.rem(s + k, n_fs)), device_id_type=MESH)
        return c

    lax.fori_loop(1, n_fs, greet, 0)
    pl.semaphore_signal(barrier, inc=1, device_id=across, device_id_type=MESH)
    pl.semaphore_signal(barrier, inc=1, device_id=partner, device_id_type=MESH)
    pl.semaphore_wait(barrier, n_fs + 1)

    last = experts - 1
    start_x1(0)
    start_z1(0)
    start_down(0)
    for e in range(1, experts):
        if e < 2:
            start_x1(e)
        start_z1(e)

    fetch = pltpu.make_async_copy(tok, nrm, lsem.at[0])
    fetch.start()
    fetch.wait()

    def norm_step(t, carry):
        at = window(t * tile_rows, tile_rows)
        values = nrm[at, :].astype(jnp.float32)
        mean = jnp.mean(values * values, axis=-1, keepdims=True)
        nrm[at, :] = (values * lax.rsqrt(mean + 1e-06)).astype(jnp.bfloat16)
        return carry

    lax.fori_loop(0, n_fs, norm_step, 0)
    for e in range(experts):
        local(down_b.at[e], dbounce, down_o.at[e, :, columns(g)])

    relay(0)
    for e in range(experts):
        collect_long(e)
        if e + 2 < experts:
            start_x1(e + 2)
        if e + 1 < experts:
            start_down(e + 1)
            relay(e + 1)
        relay_down(e)
        collect_short(e)
        load(e)
        if e < last:
            each(lambda t, e=e: tile(e, t))

    def to_pair(k):
        zt = lax.rem(z + 1 + k, n_hi)
        return remote(ysend.at[k], yrecv.at[zt], ys.at[k], yr.at[zt], along(s + 1 - 2 * y))

    def to_owner(k):
        zt = lax.rem(z + 1 + k, n_hi)
        return remote(zsend.at[k], zrecv.at[k], zs.at[k], zr.at[k], along(zt * 2 + y))

    def pair_step(k, carry):
        zt = lax.rem(z + 1 + k, n_hi)
        at = tile(last, zt * 2 + 1 - y)
        ysend[k] = total[at, :].astype(jnp.bfloat16)
        to_pair(k).start()
        return carry

    lax.fori_loop(0, n_hi, pair_step, 0)

    def owner_step(k, carry):
        zt = lax.rem(z + 1 + k, n_hi)
        at = tile(last, zt * 2 + y)
        remote(ysend.at[k], yrecv.at[zt], ys.at[k], yr.at[zt], along(s + 1 - 2 * y)).wait_recv()
        zsend[k] = (total[at, :] + yrecv[zt].astype(jnp.float32)).astype(jnp.bfloat16)
        to_owner(k).start()
        return carry

    lax.fori_loop(0, n_hi - 1, owner_step, 0)
    at = tile(last, s)
    to_pair(n_hi - 1).wait_recv()
    total[at, :] = total[at, :] + yrecv[z].astype(jnp.float32)

    def gather_step(k, carry):
        to_owner(k).wait_recv()
        total[at, :] = total[at, :] + zrecv[k].astype(jnp.float32)
        return carry

    lax.fori_loop(0, n_hi - 1, gather_step, 0)
    mout[...] = total[at, :].astype(jnp.bfloat16)
    done = pltpu.make_async_copy(mout, mixed_o, lsem.at[0])
    done.start()
    done.wait()

    for e in range(experts):
        dx(e).wait_send()
        dp(e).wait_send()
        df(e).wait_send()
        for m in range(2):
            for j in range(blocks):
                x1(e, m, j).wait_send()

                @pl.when(g * blocks + j != s)
                def _():
                    z1(e, m, j).wait_send()

                @pl.when(other * blocks + j != s)
                def _():
                    z2(e, m, j).wait_send()

            @pl.when(receives)
            def _():
                def step(k):
                    x2(e, m, k).wait_send()
                    d1(e, m, k).wait_send()
                    d2(e, m, k).wait_send()

                each(step)

    def drain_pair(k, carry):
        to_pair(k).wait_send()
        return carry

    def drain_owner(k, carry):
        to_owner(k).wait_send()
        return carry

    lax.fori_loop(0, n_hi, drain_pair, 0)
    lax.fori_loop(0, n_hi - 1, drain_owner, 0)


def make_shards(n_fs, n_group):
    def shards(tokens, gate_master, up_master, down_master, norm_gain, route, route_weight):
        experts, rows, columns = gate_master.shape
        blocks = n_fs // n_group
        width = columns // blocks
        depth = rows * n_fs
        _, count, features = tokens.shape
        high = down_master.shape[2]
        side = 16 * max(1, round(rows / 96))
        long = rows - side
        tile_rows = count // n_fs
        n_hi = n_fs // 2
        units = 2 * experts

        def cut(master):
            scaled = (norm_gain[None, :, None] * master).astype(jnp.bfloat16)
            return scaled.reshape(experts, rows, blocks, width).transpose(0, 2, 1, 3)

        gate_b, up_b = cut(gate_master), cut(up_master)
        down_b = down_master.astype(jnp.bfloat16)
        comb = mixing(route[0], route_weight[0], experts)
        bf16 = jnp.bfloat16
        fused = width % LANES == 0
        parts = width // LANES if fused else 2
        anywhere = pl.BlockSpec(memory_space=pl.ANY)
        dma = pltpu.SemaphoreType.DMA
        gate_out, up_out, down_out, mixed, _ = pl.pallas_call(
            functools.partial(kernel, n_fs, side),
            out_shape=(
                jax.ShapeDtypeStruct((experts, depth, width), bf16),
                jax.ShapeDtypeStruct((experts, depth, width), bf16),
                jax.ShapeDtypeStruct((experts, width, n_group * high), bf16),
                jax.ShapeDtypeStruct((tile_rows, features), bf16),
                jax.ShapeDtypeStruct((experts, 2, blocks, long, width), bf16),
            ),
            in_specs=[anywhere] * 4 + [pl.BlockSpec(memory_space=pltpu.VMEM)],
            out_specs=[anywhere] * 5,
            scratch_shapes=[
                pltpu.VMEM((count, features), bf16),
                pltpu.VMEM((count, features), jnp.float32),
                pltpu.VMEM((parts, depth, 2 * LANES if fused else width), bf16),
                pltpu.VMEM((width, features), bf16),
                pltpu.VMEM((tile_rows, width), bf16),
                pltpu.VMEM((long, width), bf16),
                pltpu.VMEM((width, high), bf16),
                pltpu.VMEM((n_hi, tile_rows, features), bf16),
                pltpu.VMEM((n_hi, tile_rows, features), bf16),
                pltpu.VMEM((n_hi - 1, tile_rows, features), bf16),
                pltpu.VMEM((n_hi - 1, tile_rows, features), bf16),
                pltpu.VMEM((tile_rows, features), bf16),
                dma((units, blocks)), dma((units, blocks)), dma((units, blocks)), dma((units, blocks)),
                dma((units, n_fs)), dma((units, n_fs)), dma((units, n_fs)), dma((units, n_fs)), dma((units, n_fs)),
                dma((experts,)), dma((experts,)), dma((experts,)), dma((experts,)), dma((experts,)), dma((experts,)),
                dma((n_hi,)), dma((n_hi,)), dma((n_hi,)), dma((n_hi,)),
                dma((2 + 2 * parts,)),
            ],
            compiler_params=pltpu.CompilerParams(
                collective_id=0, has_side_effects=True, vmem_limit_bytes=67043328
            ),
        )(tokens[0], gate_b, up_b, down_b, comb)
        return gate_out, up_out, down_out, mixed[None]

    return shards


def solution(mesh):
    n_fs = mesh.shape["fs"]
    n_group = mesh.shape["gr"] * mesh.shape["tp"]
    in_specs = (
        P(GROUP, None, None),
        P(None, "fs", GROUP),
        P(None, "fs", GROUP),
        P(None, "fs", GROUP),
        P("fs"),
        P(GROUP, None, None),
        P(GROUP, None, None),
    )
    out_specs = (
        P(None, None, "fs"),
        P(None, None, "fs"),
        P(None, "fs", None),
        P(GROUP, "fs", None),
    )
    return jax.shard_map(
        make_shards(n_fs, n_group), mesh=mesh, in_specs=in_specs, out_specs=out_specs, check_vma=False
    )
```

time: 623 us -> 472 us (0.76); the launches traced: 611 us -> 471 us
  Pallas kernels: 0 us -> 412 us
  waiting for transfers between devices: 240 us -> 0 us
  matrix products: 136 us -> 0 us
  starting transfers between devices: 88.4 us -> 0 us
  other arithmetic: 73.8 us -> 13.4 us
  between operations: 14.8 us -> 0.68 us
  local copies, waits for them, and re-layouts: 58 us -> 44.9 us
    pallas_call x0 -> x1, Pallas kernels: none -> 412 us  [shards(): pl.pallas_call(functools.partial(kernel, n_fs, side), out_shape=(jax.Shap...]
    dot_general x8 -> x0, matrix products: 136 us -> none  [the longest x4 87.6 us: expert_term(): projected = jnp.dot(hidden, down_weight, preferred_element_type=jnp.float32)]
    reduce_scatter x2 -> x0, waiting for transfers between devices: 129 us -> none  [shards(): lax.psum_scatter(summed, 'fs', scatter_dimension=0, tiled=True)]
    all_to_all x1 -> x0, waiting for transfers between devices: 96.3 us -> none  [shards(): pair = lax.all_to_all(pair, GROUP, split_axis=0, concat_axis=0, tiled=True)]
    ppermute x21 -> x0, starting transfers between devices: 81.3 us -> none  [permuted(): lax.ppermute(block, 'fs', [(i, (i + shift) % n_fs) for i in range(n_fs)])]
    unnamed x25 -> x18, local copies, waits for them, and re-layouts: 2.29 us -> 36.2 us
    another operation x4 -> x0, other arithmetic: 24.3 us -> none  [the longest x1 11.8 us: shards(): down_out = jnp.stack(down_list, axis=0)]
    slice x9 -> x0, local copies, waits for them, and re-layouts: 21.8 us -> none  [the longest x1 7.94 us: local(): scaled = (norm_gain[:, None] * master[index]).astype(jnp.bfloat16)]
  transfers between devices with their start and end apart: 33 -> 0, of which waited for: 10 -> 0; matrix products, arithmetic and copies ran while one was open for 39% -> 0% of each run, Pallas kernels for 0% -> 0%
where the time goes in v1:
time: 472 us; the launch traced here: 471 us
  Pallas kernels  412 us (87%)
  local copies, waits for them, and re-layouts  44.9 us (10%)
  other arithmetic  13.4 us (3%)
    pallas_call x1, Pallas kernels, shards(): pl.pallas_call(functools.partial(kernel, n_fs, side), out_shape=(jax.Shap...  412 us
    unnamed x18, local copies, waits for them, and re-layouts  36.2 us

profile of v1, /device:TPU:26, one launch (start us, length us, event | category | flops | bytes accessed | tf_op | source)
XLA Modules:
  0.0 471.4 jit_solution(6787826316787957215)
XLA Ops:
  0.6 0.7 reduce_sum.18
  1.4 0.7 bitcast_divide_fusion
  2.1 0.8 fusion
  2.9 1.3 copy.23.comb
  4.3 4.4 convert_element_type.12.down_b
  8.7 6.1 %copy.19 = f32[3,256,1792]{1,2,0:T(8,128)} copy(f32[3,256,1792]{2,1,0:T(8,128)} %param.8) | data formatting | bytes 11010048 | tf_op args[1]
  14.8 0.0 copy-start.2
  14.8 6.1 %copy.21 = f32[3,256,1792]{1,2,0:T(8,128)} copy(f32[3,256,1792]{2,1,0:T(8,128)} %param.9) | data formatting | bytes 11010048 | tf_op args[2]
  20.9 0.0 copy-done.2
  20.9 6.7 %multiply_convert_fusion = (bf16[3,256,1792]{1,2,0:T(8,128)(2,1)}, bf16[3,256,1792]{1,2,0:T(8,128)(2,1)S(1)}) fusion(f32[3,256,1792]{1,2,0:T(8,128)} %copy.21, f32[256]{0:T(256)S(1)} %copy-done.2, f32[3,256,1792]{1,2,0:T(8,128)} %copy.19), kind=kLoop, calls=%fused_computation | loop fusion | flops 5505024 | bytes 16516096 | tf_op jit(solution)/shard_map/convert_element_type | solution.py:397
  27.6 4.5 copy.22
  32.1 2.9 copy.20
  35.0 412.5 %shard_map.102 = (bf16[3,2048,896]{2,1,0:T(8,128)(2,1)}, bf16[3,2048,896]{2,1,0:T(8,128)(2,1)}, bf16[3,896,2048]{2,1,0:T(8,128)(2,1)}, bf16[256,2048]{1,0:T(8,128)(2,1)}, bf16[3,2,2,208,896]{4,3,2,1,0:T(8,128)(2,1)}) custom-call(bf16[2048,2048]{1,0:T(8,128)(2,1)} %bitcast.15, bf16[3,2,256,896]{3,2,1,0:T(8,128)(2,1)} %bitcast.12, ...), custom_call_target="tpu_custom_call" | custom-call | tf_op jit(solution)/shard_map/pallas_call | solution.py:408
  447.4 0.0 copy-start
  447.5 0.0 slice-start
  447.5 0.0 slice-start.1
  447.5 11.4 %copy.28 = bf16[3,2048,896]{2,1,0:T(8,128)(2,1)} copy(bf16[3,2048,896]{2,1,0:T(8,128)(2,1)} %get-tuple-element.18) | data formatting | bytes 22020096
  458.9 0.0 copy-done
  458.9 0.0 slice-start.2
  458.9 5.6 %copy.29 = bf16[3,2048,896]{2,1,0:T(8,128)(2,1)} copy(bf16[3,2048,896]{2,1,0:T(8,128)(2,1)S(1)} %copy-done) | data formatting | bytes 22020096
  464.4 0.0 slice-done
  464.4 0.2 slice-done.1
  464.7 1.6 slice-done.2
  466.2 0.0 copy-start.1
  466.2 4.3 copy.30
  470.5 0.0 copy-done.1
  470.5 1.0 copy.31
  (1 shorter events, 0.0 us)
Async XLA Ops:
  14.8 6.1 %copy-start.2 = (f32[256]{0:T(256)S(1)}, f32[256]{0:T(256)}, u32[]{:S(2)}) copy-start(f32[256]{0:T(256)} %param.11) | copy-start | bytes 3076
  447.4 11.4 %copy-start = (bf16[3,2048,896]{2,1,0:T(8,128)(2,1)S(1)}, bf16[3,2048,896]{2,1,0:T(8,128)(2,1)}, u32[]{:S(2)}) copy-start(bf16[3,2048,896]{2,1,0:T(8,128)(2,1)} %get-tuple-element.19) | copy-start | bytes 33030148
  447.5 17.0 %slice-start = ((s8[11010048]{0:T(1024)(128)(4,1)}), s8[4194304]{0:T(1024)(128)(4,1)S(1)}, s32[]{:S(2)}) async-start(s8[11010048]{0:T(1024)(128)(4,1)} %bitcast.9), calls=%async_computation | async-start | bytes 8388608
  447.5 17.2 %slice-start.1 = ((s8[11010048]{0:T(1024)(128)(4,1)}), s8[4194304]{0:T(1024)(128)(4,1)S(1)}, s32[]{:S(2)}) async-start(s8[11010048]{0:T(1024)(128)(4,1)} %bitcast.9), calls=%async_computation.1 | async-start | bytes 8388608
  458.9 7.3 %slice-start.2 = ((s8[11010048]{0:T(1024)(128)(4,1)}), s8[2621440]{0:T(1024)(128)(4,1)S(1)}, s32[]{:S(2)}) async-start(s8[11010048]{0:T(1024)(128)(4,1)} %bitcast.9), calls=%async_computation.2 | async-start | bytes 5242880
  466.2 4.3 copy-start.1

commit v2 on v1

v2 whole, which is shorter than its diff:
```python
import functools

import jax
import jax.numpy as jnp
from jax import lax
from jax.experimental import pallas as pl
from jax.experimental.pallas import tpu as pltpu
from jax.sharding import PartitionSpec as P

GROUP = ("gr", "tp")
MESH = pl.DeviceIdType.MESH
LANES = 128


def mixing(chosen, weights, experts):
    labels = jnp.arange(experts, dtype=jnp.int32)[None, :]
    total = weights[:, :1] + weights[:, 1:2]
    first = jnp.where(chosen[:, :1] == labels, weights[:, :1] / total, 0.0)
    second = jnp.where(chosen[:, 1:2] == labels, weights[:, 1:2] / total, 0.0)
    return first + second


def kernel(
    n_fs, sides,
    tok, gate_m, up_m, down_m, gain, comb,
    gate_o, up_o, down_o, mixed_o, stage, gate_b, up_b, down_b,
    nrm, total, w1, wd, hid, bounce, dstage, dbounce, cast, ysend, yrecv, zsend, zrecv, mout,
    x1s, x1r, z1s, z2s, rl, rs, x2s, d1s, d2s, dxs, dxr, dps, dpr, dfs, dfr, ys, yr, zs, zr, lsem, msem, wsem, dsem,
):
    gr, s, tp = lax.axis_index("gr"), lax.axis_index("fs"), lax.axis_index("tp")
    src = (gate_b, up_b)
    masters = (gate_m, up_m)
    out = (gate_o, up_o)
    experts, blocks, rows, width = gate_b.shape
    depth = n_fs * rows
    high = down_b.shape[2]
    count, features = tok.shape
    longs_of = [rows - side for side in sides]
    tile_rows = count // n_fs
    n_hi = n_fs // 2
    z, y = s // 2, s % 2

    g, other = gr * 2 + tp, (1 - gr) * 2 + tp
    home = s // blocks
    off_plane = (gr - home // 2) * (gr - home // 2)
    off_core = (tp - home % 2) * (tp - home % 2)
    receives = off_core == 0

    across = {"gr": 1 - gr, "fs": s, "tp": tp}
    partner = {"gr": gr, "fs": s, "tp": 1 - tp}
    relayer = {"gr": 1 - gr, "fs": s, "tp": 1 - home % 2}

    def along(f, core=tp):
        return {"gr": gr, "fs": f, "tp": core}

    def remote(a, b, send, recv, to):
        return pltpu.make_async_remote_copy(
            src_ref=a, dst_ref=b, send_sem=send, recv_sem=recv, device_id=to, device_id_type=MESH
        )

    def window(start, size):
        return pl.ds(pl.multiple_of(start, 16), size)

    def staged(e, m, j, core):
        return stage.at[core, e, m, j, pl.ds(0, longs_of[e])]

    def x1(e, m, j, core=tp):
        u = 2 * e + m
        return remote(
            src[m].at[e, j, pl.ds(sides[e], longs_of[e])], staged(e, m, j, core), x1s.at[u, j], x1r.at[core, u, j], relayer
        )

    def z1(e, m, j):
        u = 2 * e + m
        return remote(
            src[m].at[e, j, pl.ds(0, longs_of[e])], out[m].at[e, window(s * rows, longs_of[e])],
            z1s.at[u, j], rl.at[u, s], along(g * blocks + j),
        )

    def z2(e, m, j, core):
        u = 2 * e + m
        at = ((1 - gr) * 2 + core) * blocks + j
        return remote(
            staged(e, m, j, core), out[m].at[e, window(s * rows + sides[e], longs_of[e])],
            z2s.at[core, u, j], rl.at[u, s], along(at, core),
        )

    def long_part(e, m, at):
        return out[m].at[e, window(at * rows + sides[e] * off_plane, longs_of[e])]

    def d1(e, m, at):
        u = 2 * e + m
        part = long_part(e, m, at)
        return remote(part, part, d1s.at[u, at], rl.at[u, at], partner)

    def x2(e, m, at):
        u = 2 * e + m
        part = out[m].at[e, window(at * rows + longs_of[e] * off_plane, sides[e])]
        return remote(part, part, x2s.at[u, at], rs.at[u, at], across)

    def d2(e, m, at):
        u = 2 * e + m
        part = out[m].at[e, window(at * rows + longs_of[e] * (1 - off_plane), sides[e])]
        return remote(part, part, d2s.at[u, at], rs.at[u, at], partner)

    def columns(group):
        return pl.ds(pl.multiple_of(group * high, LANES), high)

    def dx(e):
        return remote(down_b.at[e], down_o.at[e, :, columns(g)], dxs.at[e], dxr.at[e], across)

    def dp(e):
        return remote(down_b.at[e], down_o.at[e, :, columns(g)], dps.at[e], dpr.at[e], partner)

    def df(e):
        part = down_o.at[e, :, columns(other)]
        return remote(part, part, dfs.at[e], dfr.at[e], partner)

    def each(fn):
        lax.fori_loop(0, n_fs, lambda k, c: (fn(k), c)[1], 0)

    def start_x1(e):
        for m in range(2):
            for j in range(blocks):
                x1(e, m, j).start()

    def start_down(e):
        dx(e).start()
        dp(e).start()

    def relay(e):
        for m in range(2):
            for j in range(blocks):
                for core in range(2):
                    x1(e, m, j, core).wait_recv()
                    z2(e, m, j, core).start()

    def relay_down(e):
        dx(e).wait_recv()
        df(e).start()

    def local(a, buffer, b):
        copy = pltpu.make_async_copy(a, buffer, lsem.at[0])
        copy.start()
        copy.wait()
        copy = pltpu.make_async_copy(buffer, b, lsem.at[0])
        copy.start()
        copy.wait()

    def long_step(e, k):
        at = lax.rem(s + k, n_fs)
        near = off_plane + k == 0
        for m in range(2):
            @pl.when(near)
            def _():
                local(
                    src[m].at[e, s - home * blocks, pl.ds(0, longs_of[e])],
                    bounce.at[pl.ds(0, longs_of[e])],
                    long_part(e, m, s),
                )

            @pl.when(jnp.logical_not(near))
            def _():
                d1(e, m, at).wait_recv()

            x2(e, m, at).start()
            d1(e, m, at).start()

    def short_step(e, k):
        at = lax.rem(s + k, n_fs)
        for m in range(2):
            d2(e, m, at).wait_recv()
            d2(e, m, at).start()

    def final_step(e, k):
        at = lax.rem(s + k, n_fs)
        for m in range(2):
            d1(e, m, at).wait_recv()
            d2(e, m, at).wait_recv()

    fused = width % LANES == 0

    def load(e):
        dp(e).wait_recv()
        df(e).wait_recv()
        copies = [pltpu.make_async_copy(down_o.at[e], wd, lsem.at[1])]
        if fused:
            for c in range(width // LANES):
                for m in range(2):
                    copies.append(
                        pltpu.make_async_copy(
                            out[m].at[e, :, pl.ds(c * LANES, LANES)],
                            w1.at[c, :, pl.ds(m * LANES, LANES)],
                            lsem.at[2 + 2 * c + m],
                        )
                    )
        else:
            for m in range(2):
                copies.append(pltpu.make_async_copy(out[m].at[e], w1.at[m], lsem.at[2 + m]))
        for copy in copies:
            copy.start()
        for copy in copies:
            copy.wait()

    def gated(gate_act, up_act):
        return (gate_act / (1.0 + jnp.exp(-gate_act)) * up_act).astype(jnp.bfloat16)

    def dot(a, b):
        return jnp.dot(a, b, preferred_element_type=jnp.float32)

    step_n = min(512, features)

    def tile(e, start, size, flat=False):
        at = window(start, size)
        rows_of = pl.ds(0, size)
        if fused:
            def hidden(c, carry):
                both = dot(nrm[at, :], w1[c])
                cols = pl.ds(pl.multiple_of(c * LANES, LANES), LANES)
                hid[rows_of, cols] = gated(both[:, :LANES], both[:, LANES:])
                return carry

            lax.fori_loop(0, width // LANES, hidden, 0, unroll=flat)
        else:
            hid[rows_of, :] = gated(dot(nrm[at, :], w1[0]), dot(nrm[at, :], w1[1]))

        def project(c, carry):
            cols = pl.ds(pl.multiple_of(c * step_n, LANES), step_n)
            term = comb[at, e : e + 1] * dot(hid[rows_of, :], wd[:, cols])
            total[at, cols] = term if e == 0 else total[at, cols] + term
            return carry

        lax.fori_loop(0, features // step_n, project, 0, unroll=flat)
        return at

    def read(u):
        return pltpu.make_async_copy(
            masters[u % 2].at[u // 2],
            total.at[pl.ds(u * rows, rows), pl.ds(0, blocks * width)],
            msem.at[u],
        )

    def write(u):
        return pltpu.make_async_copy(cast.at[u % 2], src[u % 2].at[u // 2], wsem.at[u % 2])

    def read_down(e):
        return pltpu.make_async_copy(down_m.at[e], dstage, dsem.at[0])

    def write_down(e):
        return (
            pltpu.make_async_copy(dbounce, down_b.at[e], dsem.at[1]),
            pltpu.make_async_copy(dbounce, down_o.at[e, :, columns(g)], dsem.at[2]),
        )

    def round_unit(u):
        read(u).wait()
        for j in range(blocks):
            part = total[pl.ds(u * rows, rows), j * width : (j + 1) * width]
            cast[u % 2, j] = (gain[...] * part).astype(jnp.bfloat16)
        write(u).start()

    def start_z1(e, m):
        for j in range(blocks):
            @pl.when(g * blocks + j != s)
            def _():
                z1(e, m, j).start()

    def release(u):
        e, m = u // 2, u % 2
        write(u).wait()
        for j in range(blocks):
            x1(e, m, j).start()
        if e == 0:
            start_z1(e, m)

    def round_down(e):
        read_down(e).wait()
        dbounce[...] = dstage[...].astype(jnp.bfloat16)
        for copy in write_down(e):
            copy.start()
        if e + 1 < experts:
            read_down(e + 1).start()
        for copy in write_down(e):
            copy.wait()

    units = 2 * experts
    for u in range(units):
        read(u).start()
    read_down(0).start()
    barrier = pltpu.get_barrier_semaphore()

    def hello(to):
        pl.semaphore_signal(barrier, inc=1, device_id=to, device_id_type=MESH)

    def greet(k, c):
        at = lax.rem(s + k, n_fs)
        hello(along(at))
        hello(along(at, 1 - tp))
        return c

    lax.fori_loop(1, n_fs, greet, 0)
    hello(partner)
    hello(across)
    hello({"gr": 1 - gr, "fs": s, "tp": 1 - tp})
    pl.semaphore_wait(barrier, 2 * n_fs + 1)

    last = experts - 1
    fetch = pltpu.make_async_copy(tok, nrm, lsem.at[0])
    fetch.start()
    early = min(2, experts)
    with jax.named_scope("cast"):
        for u in range(2 * early):
            round_unit(u)
            if u >= 1:
                release(u - 1)
        release(2 * early - 1)
        round_down(0)
        start_down(0)

    def norm_step(t, carry):
        at = window(t * tile_rows, tile_rows)
        values = nrm[at, :].astype(jnp.float32)
        mean = jnp.mean(values * values, axis=-1, keepdims=True)
        nrm[at, :] = (values * lax.rsqrt(mean + 1e-06)).astype(jnp.bfloat16)
        return carry

    def late():
        with jax.named_scope("late"):
            for u in range(2 * early, units):
                round_unit(u)
                write(u).wait()
            for e in range(1, experts):
                round_down(e)
            fetch.wait()
            lax.fori_loop(0, n_fs, norm_step, 0)

    big = 2 * tile_rows

    def more_x(e):
        if e + 2 < experts:
            start_x1(e + 2)

    def more_down(e):
        if e + 1 < experts:
            start_down(e + 1)

    def open_z(e):
        if 0 < e < experts:
            for m in range(2):
                start_z1(e, m)

    def longs(e, start, stop):
        with jax.named_scope(f"long{e}"):
            lax.fori_loop(start, stop, lambda k, c: (long_step(e, k), c)[1], 0)

    def shorts(e):
        with jax.named_scope(f"rdown{e}"):
            relay_down(e)
        with jax.named_scope(f"short{e}"):
            each(lambda k: short_step(e, k))

    half_fs = n_fs // 2
    for e in range(experts):
        @pl.when(receives)
        def _(e=e):
            if e == 0:
                late()
                open_z(1)
                longs(0, 0, half_fs)
                longs(0, half_fs, n_fs)
                more_x(0)
                more_down(0)
                open_z(2)
                if experts > 2:
                    longs(1, 0, half_fs)
            shorts(e)
            if e == 0:
                if experts > 2:
                    longs(1, half_fs, n_fs)
            else:
                more_x(e)
                more_down(e)
                open_z(e + 2)

        @pl.when(off_core != 0)
        def _(e=e):
            if e == 0:
                for ahead in range(experts):
                    with jax.named_scope(f"relay{ahead}"):
                        relay(ahead)
                    if ahead == 0:
                        open_z(1)
                        late()
                    else:
                        if ahead == 1:
                            with jax.named_scope("rdown0"):
                                relay_down(0)
                        open_z(ahead + 1)
                    more_x(ahead)
                    if ahead == 0:
                        more_down(0)
            else:
                more_down(e)
                with jax.named_scope(f"rdown{e}"):
                    relay_down(e)
            with jax.named_scope(f"final{e}"):
                each(lambda k: final_step(e, k))

        with jax.named_scope(f"load{e}"):
            load(e)
        if e < last:
            follow = e + 1 if experts == 2 or e > 0 else experts

            def both(t, carry, e=e, follow=follow):
                tile(e, t * big, big, True)
                if follow < experts:
                    @pl.when(receives)
                    def _():
                        long_step(follow, 2 * t)
                        long_step(follow, 2 * t + 1)

                return carry

            with jax.named_scope(f"dots{e}"):
                lax.fori_loop(0, half_fs, both, 0)

    half = n_hi // 2
    upper = z // half
    step_h = features // 2

    def turn(k):
        crossing = 1 - k // half
        return (upper + crossing * (1 - 2 * upper)) * half + (z + 1 + k) % half

    def to_pair(k, h):
        zt = turn(k)
        return remote(ysend.at[k, h], yrecv.at[zt, h], ys.at[k, h], yr.at[zt, h], along(s + 1 - 2 * y))

    def to_owner(k, h, cross=False):
        zt = (1 - upper) * half + z % half if cross else upper * half + (z + 1 + k) % half
        return remote(zsend.at[k, h], zrecv.at[k, h], zs.at[k, h], zr.at[k, h], along(zt * 2 + y))

    def pair_step(k, carry):
        at = tile(last, (turn(k) * 2 + 1 - y) * tile_rows, tile_rows)
        for h in range(2):
            ysend[k, h] = total[at, h * step_h : (h + 1) * step_h].astype(jnp.bfloat16)
            to_pair(k, h).start()
        return carry

    def summed(at, k, h):
        to_pair(k, h).wait_recv()
        return total[at, h * step_h : (h + 1) * step_h] + yrecv[turn(k), h].astype(jnp.float32)

    def drain_weights():
        for e in range(experts):
            dx(e).wait_send()
            dp(e).wait_send()
            df(e).wait_send()
            for m in range(2):
                for j in range(blocks):
                    x1(e, m, j).wait_send()

                    @pl.when(g * blocks + j != s)
                    def _():
                        z1(e, m, j).wait_send()

                    @pl.when(off_core != 0)
                    def _():
                        for core in range(2):
                            z2(e, m, j, core).wait_send()

                @pl.when(receives)
                def _():
                    def step(k):
                        x2(e, m, k).wait_send()
                        d1(e, m, k).wait_send()
                        d2(e, m, k).wait_send()

                    each(step)

    def halves(h):
        return slice(h * step_h, (h + 1) * step_h)

    def add_arrived(at, h, start, stop):
        def step(k, carry):
            to_owner(k, h).wait_recv()
            total[at, halves(h)] = total[at, halves(h)] + zrecv[k, h].astype(jnp.float32)
            return carry

        lax.fori_loop(start, stop, step, 0)

    def owner_step(k, cross):
        at = tile(last, (turn(k) * 2 + y) * tile_rows, tile_rows)
        for h in range(2):
            if cross:
                total[at, halves(h)] = summed(at, k, h)
                add_arrived(at, h, 0, half - 1)
                zsend[k, h] = total[at, halves(h)].astype(jnp.bfloat16)
            else:
                zsend[k, h] = summed(at, k, h).astype(jnp.bfloat16)
            to_owner(k, h, cross).start()

    def owners(start, stop, cross, lead):
        def step(k, carry):
            if lead:
                pair_step(k + lead, carry)
            owner_step(k, cross)
            return carry

        if stop > start:
            lax.fori_loop(start, stop, step, 0)

    lead = min(2, n_hi - half)
    with jax.named_scope("pairs"):
        lax.fori_loop(0, lead, pair_step, 0)
    with jax.named_scope("owners"):
        owners(0, half - 1, False, lead)
        owners(half - 1, half, True, lead)
        owners(half, n_hi - lead, False, lead)
        owners(n_hi - lead, n_hi - 1, False, 0)
    drain_weights()
    with jax.named_scope("own"):
        at = tile(last, s * tile_rows, tile_rows)
        for h in range(2):
            total[at, halves(h)] = summed(at, n_hi - 1, h)
            add_arrived(at, h, half - 1, n_hi - 1)
    mout[...] = total[at, :].astype(jnp.bfloat16)
    done = pltpu.make_async_copy(mout, mixed_o, lsem.at[0])
    done.start()
    done.wait()

    def drain_pair(k, carry):
        for h in range(2):
            to_pair(k, h).wait_send()
        return carry

    def drain_owner(k, carry):
        for h in range(2):
            to_owner(k, h).wait_send()
        return carry

    lax.fori_loop(0, n_hi, drain_pair, 0)
    lax.fori_loop(0, n_hi - 1, drain_owner, 0)


def make_shards(n_fs, n_group):
    def shards(tokens, gate_master, up_master, down_master, norm_gain, route, route_weight):
        experts, rows, columns = gate_master.shape
        blocks = n_fs // n_group
        width = columns // blocks
        depth = rows * n_fs
        _, count, features = tokens.shape
        high = down_master.shape[2]
        shares = (4, 6) + (2,) * experts
        sides = tuple(16 * max(1, rows * shares[e] // 256) for e in range(experts))
        long = rows - min(sides)
        tile_rows = count // n_fs
        n_hi = n_fs // 2
        units = 2 * experts

        comb = mixing(route[0], route_weight[0], experts)
        bf16 = jnp.bfloat16
        fused = width % LANES == 0
        parts = width // LANES if fused else 2
        anywhere = pl.BlockSpec(memory_space=pl.ANY)
        dma = pltpu.SemaphoreType.DMA
        gate_out, up_out, down_out, mixed, *_ = pl.pallas_call(
            functools.partial(kernel, n_fs, sides),
            out_shape=(
                jax.ShapeDtypeStruct((experts, depth, width), bf16),
                jax.ShapeDtypeStruct((experts, depth, width), bf16),
                jax.ShapeDtypeStruct((experts, width, n_group * high), bf16),
                jax.ShapeDtypeStruct((tile_rows, features), bf16),
                jax.ShapeDtypeStruct((2, experts, 2, blocks, long, width), bf16),
                jax.ShapeDtypeStruct((experts, blocks, rows, width), bf16),
                jax.ShapeDtypeStruct((experts, blocks, rows, width), bf16),
                jax.ShapeDtypeStruct((experts, width, high), bf16),
            ),
            in_specs=[anywhere] * 4 + [pl.BlockSpec(memory_space=pltpu.VMEM)] * 2,
            out_specs=[anywhere] * 8,
            scratch_shapes=[
                pltpu.VMEM((count, features), bf16),
                pltpu.VMEM((count, features), jnp.float32),
                pltpu.VMEM((parts, depth, 2 * LANES if fused else width), bf16),
                pltpu.VMEM((width, features), bf16),
                pltpu.VMEM((2 * tile_rows, width), bf16),
                pltpu.VMEM((long, width), bf16),
                pltpu.VMEM((width, high), jnp.float32),
                pltpu.VMEM((width, high), bf16),
                pltpu.VMEM((2, blocks, rows, width), bf16),
                pltpu.VMEM((n_hi, 2, tile_rows, features // 2), bf16),
                pltpu.VMEM((n_hi, 2, tile_rows, features // 2), bf16),
                pltpu.VMEM((n_hi - 1, 2, tile_rows, features // 2), bf16),
                pltpu.VMEM((n_hi - 1, 2, tile_rows, features // 2), bf16),
                pltpu.VMEM((tile_rows, features), bf16),
                dma((units, blocks)), dma((2, units, blocks)), dma((units, blocks)), dma((2, units, blocks)),
                dma((units, n_fs)), dma((units, n_fs)), dma((units, n_fs)), dma((units, n_fs)), dma((units, n_fs)),
                dma((experts,)), dma((experts,)), dma((experts,)), dma((experts,)), dma((experts,)), dma((experts,)),
                dma((n_hi, 2)), dma((n_hi, 2)), dma((n_hi, 2)), dma((n_hi, 2)),
                dma((2 + 2 * parts,)), dma((units,)), dma((2,)), dma((3,)),
            ],
            compiler_params=pltpu.CompilerParams(
                collective_id=0, has_side_effects=True, vmem_limit_bytes=67043328
            ),
        )(tokens[0], gate_master, up_master, down_master, norm_gain[:, None], comb)
        return gate_out, up_out, down_out, mixed[None]

    return shards


def solution(mesh):
    n_fs = mesh.shape["fs"]
    n_group = mesh.shape["gr"] * mesh.shape["tp"]
    in_specs = (
        P(GROUP, None, None),
        P(None, "fs", GROUP),
        P(None, "fs", GROUP),
        P(None, "fs", GROUP),
        P("fs"),
        P(GROUP, None, None),
        P(GROUP, None, None),
    )
    out_specs = (
        P(None, None, "fs"),
        P(None, None, "fs"),
        P(None, "fs", None),
        P(GROUP, "fs", None),
    )
    return jax.shard_map(
        make_shards(n_fs, n_group), mesh=mesh, in_specs=in_specs, out_specs=out_specs, check_vma=False
    )
```

time: 472 us -> 384 us (0.81)
  Pallas kernels: 412 us -> 351 us
  local copies, waits for them, and re-layouts: 44.9 us -> 26.3 us
  other arithmetic: 13.4 us -> 3.39 us
    pallas_call x1, Pallas kernels: 412 us -> 351 us  [shards(): pl.pallas_call(functools.partial(kernel, n_fs, sides), out_shape=(jax.Sha...]
    unnamed x18 -> x14, local copies, waits for them, and re-layouts: 36.2 us -> 24 us
    convert_element_type x2 -> x0, other arithmetic: 11.1 us -> none  [the longest x1 6.68 us: cut(): scaled = (norm_gain[None, :, None] * master).astype(jnp.bfloat16)]
    reshape x2 -> x0, local copies, waits for them, and re-layouts: 7.38 us -> none  [cut(): return scaled.reshape(experts, rows, blocks, width).transpose(0, 2, 1, 3)]
where the time goes in v2:
time: 384 us; the launch traced here: 382 us
  Pallas kernels  351 us (91%)
  local copies, waits for them, and re-layouts  26.3 us (7%)
    pallas_call x1, Pallas kernels, shards(): pl.pallas_call(functools.partial(kernel, n_fs, sides), out_shape=(jax.Sha...  351 us
    unnamed x14, local copies, waits for them, and re-layouts  24 us

profile of v2, /device:TPU:26, one launch (start us, length us, event | category | flops | bytes accessed | tf_op | source)
XLA Modules:
  0.0 381.7 jit_solution(11876725441911608389)
XLA Ops:
  0.6 0.8 fusion
  1.4 0.8 add_divide_fusion.1
  2.3 1.5 copy.11.gain
  3.7 2.6 select_add_fusion.comb
  6.3 351.3 %shard_map.102 = (bf16[3,2048,896]{2,1,0:T(8,128)(2,1)}, bf16[3,2048,896]{2,1,0:T(8,128)(2,1)}, bf16[3,896,2048]{2,1,0:T(8,128)(2,1)}, bf16[256,2048]{1,0:T(8,12...) custom-call(bf16[2048,2048]{1,0:T(8,128)(2,1)} %bitcast.11, ...), custom_call_target="tpu_custom_call" | custom-call | tf_op jit(solution)/shard_map/pallas_call | solution.py:567
  357.7 0.0 copy-start
  357.7 0.0 slice-start
  357.7 0.0 slice-start.1
  357.7 11.4 %copy.16 = bf16[3,2048,896]{2,1,0:T(8,128)(2,1)} copy(bf16[3,2048,896]{2,1,0:T(8,128)(2,1)} %get-tuple-element.20) | data formatting | bytes 22020096
  369.1 0.0 copy-done
  369.1 0.0 slice-start.2
  369.1 5.6 %copy.17 = bf16[3,2048,896]{2,1,0:T(8,128)(2,1)} copy(bf16[3,2048,896]{2,1,0:T(8,128)(2,1)S(1)} %copy-done) | data formatting | bytes 22020096
  374.7 0.0 slice-done
  374.7 0.2 slice-done.1
  374.9 1.6 slice-done.2
  376.4 0.0 copy-start.1
  376.4 4.3 %copy.18 = bf16[3,896,2048]{2,1,0:T(8,128)(2,1)} copy(bf16[3,896,2048]{2,1,0:T(8,128)(2,1)S(1)} %bitcast.10) | data formatting | bytes 22020096
  380.7 0.0 copy-done.1
  380.7 1.0 copy.19
  (1 shorter events, 0.0 us)
Async XLA Ops:
  357.7 11.4 %copy-start = (bf16[3,2048,896]{2,1,0:T(8,128)(2,1)S(1)}, bf16[3,2048,896]{2,1,0:T(8,128)(2,1)}, u32[]{:S(2)}) copy-start(bf16[3,2048,896]{2,1,0:T(8,128)(2,1)} %get-tuple-element.21) | copy-start | bytes 33030148
  357.7 17.0 %slice-start = ((s8[11010048]{0:T(1024)(128)(4,1)}), s8[4194304]{0:T(1024)(128)(4,1)S(1)}, s32[]{:S(2)}) async-start(s8[11010048]{0:T(1024)(128)(4,1)} %bitcast.9), calls=%async_computation | async-start | bytes 8388608
  357.7 17.2 %slice-start.1 = ((s8[11010048]{0:T(1024)(128)(4,1)}), s8[4194304]{0:T(1024)(128)(4,1)S(1)}, s32[]{:S(2)}) async-start(s8[11010048]{0:T(1024)(128)(4,1)} %bitcast.9), calls=%async_computation.1 | async-start | bytes 8388608
  369.1 7.3 %slice-start.2 = ((s8[11010048]{0:T(1024)(128)(4,1)}), s8[2621440]{0:T(1024)(128)(4,1)S(1)}, s32[]{:S(2)}) async-start(s8[11010048]{0:T(1024)(128)(4,1)} %bitcast.9), calls=%async_computation.2 | async-start | bytes 5242880
  376.4 4.3 %copy-start.1 = (bf16[256,2048]{1,0:T(8,128)(2,1)S(1)}, bf16[256,2048]{1,0:T(8,128)(2,1)}, u32[]{:S(2)}) copy-start(bf16[256,2048]{1,0:T(8,128)(2,1)} %get-tuple-element.11) | copy-start | bytes 3145732

commit v3 on v2

--- a/solution.py
+++ b/solution.py
@@ -12,19 +12,11 @@
 LANES = 128
 
 
-def mixing(chosen, weights, experts):
-    labels = jnp.arange(experts, dtype=jnp.int32)[None, :]
-    total = weights[:, :1] + weights[:, 1:2]
-    first = jnp.where(chosen[:, :1] == labels, weights[:, :1] / total, 0.0)
-    second = jnp.where(chosen[:, 1:2] == labels, weights[:, 1:2] / total, 0.0)
-    return first + second
-
-
 def kernel(
     n_fs, sides,
-    tok, gate_m, up_m, down_m, gain, comb,
+    tok, gate_m, up_m, down_m, gain_row, route, weight,
     gate_o, up_o, down_o, mixed_o, stage, gate_b, up_b, down_b,
-    nrm, total, w1, wd, hid, bounce, dstage, dbounce, cast, ysend, yrecv, zsend, zrecv, mout,
+    gain, comb, nrm, total, w1, wd, hid, bounce, dstage, dbounce, cast, ysend, yrecv, zsend, zrecv, mout,
     x1s, x1r, z1s, z2s, rl, rs, x2s, d1s, d2s, dxs, dxr, dps, dpr, dfs, dfr, ys, yr, zs, zr, lsem, msem, wsem, dsem,
 ):
     gr, s, tp = lax.axis_index("gr"), lax.axis_index("fs"), lax.axis_index("tp")
@@ -256,7 +248,7 @@
         read(u).wait()
         for j in range(blocks):
             part = total[pl.ds(u * rows, rows), j * width : (j + 1) * width]
-            cast[u % 2, j] = (gain[...] * part).astype(jnp.bfloat16)
+            cast[u % 2, j] = (gain[:, :1] * part).astype(jnp.bfloat16)
         write(u).start()
 
     def start_z1(e, m):
@@ -286,6 +278,10 @@
     units = 2 * experts
     for u in range(units):
         read(u).start()
+    if gain.shape[0] % LANES == 0:
+        gain[...] = jnp.broadcast_to(gain_row[...], (8, gain.shape[0])).T
+    else:
+        gain[...] = jnp.broadcast_to(gain_row[...], gain.shape)
     read_down(0).start()
     barrier = pltpu.get_barrier_semaphore()
 
@@ -331,6 +327,11 @@
                 write(u).wait()
             for e in range(1, experts):
                 round_down(e)
+            sums = weight[:1, :] + weight[1:2, :]
+            first, second = weight[:1, :] / sums, weight[1:2, :] / sums
+            label = lax.broadcasted_iota(jnp.int32, (8, count), 0)
+            mix = jnp.where(route[:1, :] == label, first, 0.0) + jnp.where(route[1:2, :] == label, second, 0.0)
+            comb[...] = mix.T
             fetch.wait()
             lax.fori_loop(0, n_fs, norm_step, 0)
 
@@ -558,7 +559,8 @@
         n_hi = n_fs // 2
         units = 2 * experts
 
-        comb = mixing(route[0], route_weight[0], experts)
+        aligned = rows % LANES == 0
+        gain = norm_gain[None, :] if aligned else norm_gain[:, None]
         bf16 = jnp.bfloat16
         fused = width % LANES == 0
         parts = width // LANES if fused else 2
@@ -576,9 +578,11 @@
                 jax.ShapeDtypeStruct((experts, blocks, rows, width), bf16),
                 jax.ShapeDtypeStruct((experts, width, high), bf16),
             ),
-            in_specs=[anywhere] * 4 + [pl.BlockSpec(memory_space=pltpu.VMEM)] * 2,
+            in_specs=[anywhere] * 4 + [pl.BlockSpec(memory_space=pltpu.VMEM)] * 3,
             out_specs=[anywhere] * 8,
             scratch_shapes=[
+                pltpu.VMEM((rows, 8), jnp.float32),
+                pltpu.VMEM((count, 8), jnp.float32),
                 pltpu.VMEM((count, features), bf16),
                 pltpu.VMEM((count, features), jnp.float32),
                 pltpu.VMEM((parts, depth, 2 * LANES if fused else width), bf16),
@@ -602,7 +606,7 @@
             compiler_params=pltpu.CompilerParams(
                 collective_id=0, has_side_effects=True, vmem_limit_bytes=67043328
             ),
-        )(tokens[0], gate_master, up_master, down_master, norm_gain[:, None], comb)
+        )(tokens[0], gate_master, up_master, down_master, gain, route[0].T, route_weight[0].T)
         return gate_out, up_out, down_out, mixed[None]
 
     return shards

time: 384 us -> 378 us (0.984)
  no operation moved by 1% of the time
where the time goes in v3:
time: 378 us; the launch traced here: 376 us
  Pallas kernels  351 us (93%)
  local copies, waits for them, and re-layouts  24 us (6%)
    pallas_call x1, Pallas kernels, shards(): pl.pallas_call(functools.partial(kernel, n_fs, sides), out_shape=(jax.Sha...  351 us
    unnamed x14, local copies, waits for them, and re-layouts  24 us

profile of v3, /device:TPU:26, one launch (start us, length us, event | category | flops | bytes accessed | tf_op | source)
XLA Modules:
  0.0 375.7 jit_solution(12319001994093225984)
XLA Ops:
  0.6 351.0 %shard_map.102 = (bf16[3,2048,896]{2,1,0:T(8,128)(2,1)}, bf16[3,2048,896]{2,1,0:T(8,128)(2,1)}, bf16[3,896,2048]{2,1,0:T(8,128)(2,1)}, bf16[256,2048]{1,0:T(8,12...) custom-call(bf16[2048,2048]{1,0:T(8,128)(2,1)} %bitcast.11, ...), custom_call_target="tpu_custom_call" | custom-call | tf_op jit(solution)/shard_map/pallas_call | solution.py:569
  351.7 0.0 copy-start
  351.7 0.0 slice-start
  351.7 0.0 slice-start.1
  351.7 11.4 %copy.15 = bf16[3,2048,896]{2,1,0:T(8,128)(2,1)} copy(bf16[3,2048,896]{2,1,0:T(8,128)(2,1)} %get-tuple-element.16) | data formatting | bytes 22020096
  363.1 0.0 copy-done
  363.1 0.0 slice-start.2
  363.1 5.6 %copy.16 = bf16[3,2048,896]{2,1,0:T(8,128)(2,1)} copy(bf16[3,2048,896]{2,1,0:T(8,128)(2,1)S(1)} %copy-done) | data formatting | bytes 22020096
  368.7 0.0 slice-done
  368.7 0.2 slice-done.1
  368.9 1.6 slice-done.2
  370.4 0.0 copy-start.1
  370.5 4.3 %copy.17 = bf16[3,896,2048]{2,1,0:T(8,128)(2,1)} copy(bf16[3,896,2048]{2,1,0:T(8,128)(2,1)S(1)} %bitcast.10) | data formatting | bytes 22020096
  374.7 0.0 copy-done.1
  374.7 1.0 copy.18
  (1 shorter events, 0.0 us)
Async XLA Ops:
  351.7 11.4 %copy-start = (bf16[3,2048,896]{2,1,0:T(8,128)(2,1)S(1)}, bf16[3,2048,896]{2,1,0:T(8,128)(2,1)}, u32[]{:S(2)}) copy-start(bf16[3,2048,896]{2,1,0:T(8,128)(2,1)} %get-tuple-element.17) | copy-start | bytes 33030148
  351.7 17.0 %slice-start = ((s8[11010048]{0:T(1024)(128)(4,1)}), s8[4194304]{0:T(1024)(128)(4,1)S(1)}, s32[]{:S(2)}) async-start(s8[11010048]{0:T(1024)(128)(4,1)} %bitcast.9), calls=%async_computation | async-start | bytes 8388608
  351.7 17.2 %slice-start.1 = ((s8[11010048]{0:T(1024)(128)(4,1)}), s8[4194304]{0:T(1024)(128)(4,1)S(1)}, s32[]{:S(2)}) async-start(s8[11010048]{0:T(1024)(128)(4,1)} %bitcast.9), calls=%async_computation.1 | async-start | bytes 8388608
  363.1 7.3 %slice-start.2 = ((s8[11010048]{0:T(1024)(128)(4,1)}), s8[2621440]{0:T(1024)(128)(4,1)S(1)}, s32[]{:S(2)}) async-start(s8[11010048]{0:T(1024)(128)(4,1)} %bitcast.9), calls=%async_computation.2 | async-start | bytes 5242880
  370.4 4.3 %copy-start.1 = (bf16[256,2048]{1,0:T(8,128)(2,1)S(1)}, bf16[256,2048]{1,0:T(8,128)(2,1)}, u32[]{:S(2)}) copy-start(bf16[256,2048]{1,0:T(8,128)(2,1)} %get-tuple-element.11) | copy-start | bytes 3145732
